TPU v7x, 32 devices: a whole 2x2x4 slice. The times are simulated.
32 devices in a mesh: grp: 2 (over y), sp: 4 (over z), dp: 4 (over x, core).
Axes of the slice: x: 2, y: 2, z: 4, core: 2. Of those that a mesh axis runs over, the one named last changes fastest.
Arguments:
- query_rows: bfloat16 [8, 512, 2048], P(('grp', 'dp'), 'sp'), parts along dimension 0, may hold values from -6 to 6
- key_rows: bfloat16 [8, 512, 2048], P(('grp', 'dp'), 'sp'), parts along dimension 0, may hold values from -6 to 6
- value_rows: bfloat16 [8, 512, 2048], P(('grp', 'dp'), 'sp'), parts along dimension 0, may hold values from -6 to 6
- query_gain: float32 [64], replicated, may hold values from 1.1 to 7
- key_gain: float32 [64], replicated, may hold values from 1.1 to 7
- lambdas: float32 [16], replicated, may hold values from 0.3 to 0.8
- head_gain: float32 [128], replicated, may hold values from 0.1 to 1.9
- out_weight: bfloat16 [2048, 2048], P(None, 'dp'), may hold values from -0.125 to 0.125
Outputs:
- attended: bfloat16 [8, 512, 2048], P(('grp', 'dp'), 'sp'), parts along dimension 0
There are 2 independent parts, one for each index of `grp`. A program takes and returns all parts, laid end to end along the dimension named above; an argument that names none is the same for every part. Nothing has to cross between parts.
All inputs are finite; a program needn't handle non-finite values.
Results may differ from a plain program's by a relative error of at most 0.008.
The roundings to bfloat16 on the way count: a program that leaves them out, or rounds other values in their place, can miss the bound.
Values may be sent and summed in bfloat16 or wider, within the bound.
No kernel may reach another device: no remote copies, remote signals or barrier semaphores. Data moves between devices by JAX's collectives and lax.ppermute only.
A program may use at most 128 MiB of HBM per device.

v0:
```python
import jax
import jax.numpy as jnp
from jax import lax
from jax.sharding import PartitionSpec as P

EPSILON = 1e-06
OUT_SCALE = 0.8


def norm_rotate(field_rows, gain_vector, positions):
    widened = field_rows.astype(jnp.float32)
    normed = (
        widened
        * lax.rsqrt(jnp.mean(widened * widened, axis=-1, keepdims=True) + EPSILON)
        * gain_vector
    )
    half_size = field_rows.shape[-1] // 2
    inverse = 10000.0 ** (-jnp.arange(half_size, dtype=jnp.float32) / half_size)
    angles = (positions[:, None] * inverse[None, :]).reshape(positions.shape[0], 1, 1, half_size)
    cosine_part = jnp.cos(angles)
    sine_part = jnp.sin(angles)
    first_half = normed[..., :half_size]
    second_half = normed[..., half_size:]
    turned = jnp.concatenate(
        [
            first_half * cosine_part - second_half * sine_part,
            second_half * cosine_part + first_half * sine_part,
        ],
        axis=-1,
    )
    return turned.astype(jnp.bfloat16)


def head_norm(raw_heads, gain_vector):
    scaled = raw_heads * lax.rsqrt(
        jnp.mean(raw_heads * raw_heads, axis=-1, keepdims=True) + EPSILON
    )
    return (scaled * gain_vector * OUT_SCALE).astype(jnp.bfloat16)


def block_size():
    return 512


def attend(query_head, key_head, value_head, weight_two, gain_vector):
    length = query_head.shape[0]
    block_rows = block_size()
    score_scale = query_head.shape[-1] ** (-0.5)
    offsets = jnp.arange(block_rows, dtype=jnp.int32)
    value_size = value_head.shape[-1]

    def one_block(number):
        first_row = number * block_rows
        query_block = lax.dynamic_slice_in_dim(query_head, first_row, block_rows, 0)
        query_positions = first_row + offsets

        def fill_scores(kblock, buffer):
            key_block = lax.dynamic_slice_in_dim(key_head, kblock * block_rows, block_rows, 0)
            scores = (
                jnp.einsum(
                    "qcd,kcd->cqk", query_block, key_block, preferred_element_type=jnp.float32
                )
                * score_scale
            )
            visible = (kblock * block_rows + offsets)[None, :] <= query_positions[:, None]
            scores = jnp.where(visible[None], scores, -1e30)
            return lax.dynamic_update_slice_in_dim(buffer, scores, kblock * block_rows, 2)

        start_buffer = jnp.full((2, block_rows, length), -1e30, jnp.float32)
        stored = lax.fori_loop(0, number + 1, fill_scores, start_buffer)
        highest = jnp.max(stored, axis=-1)
        totals = jnp.sum(jnp.exp(stored - highest[..., None]), axis=-1)

        def weigh_values(kblock, accumulated):
            scores = lax.dynamic_slice_in_dim(stored, kblock * block_rows, block_rows, 2)
            probabilities = jnp.exp(scores - highest[..., None]) / totals[..., None]
            mixing = (probabilities[0] - weight_two * probabilities[1]).astype(jnp.bfloat16)
            value_block = lax.dynamic_slice_in_dim(value_head, kblock * block_rows, block_rows, 0)
            return accumulated + jnp.dot(mixing, value_block, preferred_element_type=jnp.float32)

        return lax.fori_loop(
            0, number + 1, weigh_values, jnp.zeros((block_rows, value_size), jnp.float32)
        )

    blocks = lax.map(one_block, jnp.arange(length // block_rows, dtype=jnp.int32))
    return head_norm(blocks.reshape(length, value_size), gain_vector)


def local(query_rows, key_rows, value_rows, query_gain, key_gain, lambdas, head_gain, out_weight):
    tok_count = query_rows.shape[1]
    group_size = lax.axis_size("sp")
    head_size = query_gain.shape[0]
    value_size = head_gain.shape[0]
    heads_total = lambdas.shape[0]
    local_heads = heads_total // group_size

    def by_peer(tensor):
        return tensor.reshape(1, tok_count, group_size, tensor.shape[2] // group_size)

    query_in, key_in, value_in = (
        lax.all_to_all(by_peer(query_rows), "sp", split_axis=2, concat_axis=1, tiled=True),
        lax.all_to_all(by_peer(key_rows), "sp", split_axis=2, concat_axis=1, tiled=True),
        lax.all_to_all(by_peer(value_rows), "sp", split_axis=2, concat_axis=1, tiled=True),
    )
    length = tok_count * group_size
    positions = jnp.arange(length, dtype=jnp.float32)
    query_rot = norm_rotate(
        query_in.reshape(length, local_heads, 2, head_size), query_gain, positions
    )
    key_rot = norm_rotate(key_in.reshape(length, local_heads, 2, head_size), key_gain, positions)
    value_heads = value_in.reshape(length, local_heads, value_size)
    local_lambdas = lax.dynamic_slice_in_dim(
        lambdas, lax.axis_index("sp") * local_heads, local_heads
    )

    def per_head(head_index):
        return attend(
            query_rot[:, head_index],
            key_rot[:, head_index],
            value_heads[:, head_index],
            local_lambdas[head_index],
            head_gain,
        )

    outputs = lax.map(per_head, jnp.arange(local_heads, dtype=jnp.int32))
    outputs = jnp.transpose(outputs, (1, 0, 2)).reshape(1, length, 1, local_heads * value_size)
    returned = lax.all_to_all(outputs, "sp", split_axis=1, concat_axis=2, tiled=True)
    heads_rows = returned.reshape(tok_count, heads_total * value_size)
    attended = jnp.dot(
        heads_rows,
        lax.all_gather(out_weight, "dp", axis=1, tiled=True),
        preferred_element_type=jnp.float32,
    )
    return attended.astype(jnp.bfloat16).reshape(1, tok_count, attended.shape[1])


def solution(mesh):
    placed = (
        P(("grp", "dp"), "sp", None),
        P(("grp", "dp"), "sp", None),
        P(("grp", "dp"), "sp", None),
        P(),
        P(),
        P(),
        P(),
        P(None, "dp"),
    )
    return jax.shard_map(
        local, mesh=mesh, in_specs=placed, out_specs=P(("grp", "dp"), "sp", None), check_vma=False
    )
```

profile of v0, /device:TPU:0, one launch (start us, length us, event | category | flops | bytes accessed | tf_op | source)
XLA Modules:
  0.0 130.4 jit_solution(3775947803156317788)
XLA Ops:
  6.5 0.7 all-gather.2.cloned.1.call-update
  7.3 0.3 copy-done.1
  7.6 1.0 copy.25
  8.6 6.3 %all-to-all-start = ((bf16[1,128,4,512]{1,3,0,2:T(8,128)(2,1)}), bf16[1,128,4,512]{1,3,0,2:T(8,128)(2,1)S(1)}, u32[]{:S(2)}, u32[]{:S(2)}) async-start(bf16[1,128,4,512]{1,3,0,2:T(8,128)(2,1)} %bitcast.7), calls=%async_computation | async-start | bytes 1048576 | tf_op jit(solution)/shard_map/all_to_all | solution.py:102
  15.0 1.0 copy.27
  16.0 13.5 %all-to-all-done = bf16[1,128,4,512]{1,3,0,2:T(8,128)(2,1)S(1)} async-done(((bf16[1,128,4,512]{1,3,0,2:T(8,128)(2,1)}), bf16[1,128,4,512]{1,3,0,2:T(8,128)(2,1)S(1)}, u32[]{:S(2)}, u32[]{:S(2)}) %all-to-all-start) | async-done | bytes 524320 | tf_op jit(solution)/shard_map/all_to_all | solution.py:102
  29.5 3.6 %all-to-all-start.1 = ((bf16[1,128,4,512]{1,3,0,2:T(8,128)(2,1)}), bf16[1,128,4,512]{1,3,0,2:T(8,128)(2,1)S(1)}, u32[]{:S(2)}, u32[]{:S(2)}) async-start(bf16[1,128,4,512]{1,3,0,2:T(8,128)(2,1)} %bitcast.10), calls=%async_computation.1 | async-start | bytes 1048576 | tf_op jit(solution)/shard_map/all_to_all | solution.py:101
  33.1 0.3 copy.29
  33.4 1.1 copy.30
  34.4 12.7 %all-to-all-done.1 = bf16[1,128,4,512]{1,3,0,2:T(8,128)(2,1)S(1)} async-done(((bf16[1,128,4,512]{1,3,0,2:T(8,128)(2,1)}), bf16[1,128,4,512]{1,3,0,2:T(8,128)(2,1)S(1)}, u32[]{:S(2)}, u32[]{:S(2)}) %all-to-all-start.1) | async-done | bytes 524320 | tf_op jit(solution)/shard_map/all_to_all | solution.py:101
  47.1 4.1 %all-to-all-start.2 = ((bf16[1,128,4,512]{3,1,0,2:T(8,128)(2,1)}), bf16[1,128,4,512]{3,1,0,2:T(8,128)(2,1)}, u32[]{:S(2)}, u32[]{:S(2)}) async-start(bf16[1,128,4,512]{3,1,0,2:T(8,128)(2,1)} %copy.30), calls=%async_computation.2 | async-start | bytes 1048576 | tf_op jit(solution)/shard_map/all_to_all | solution.py:103
  51.3 0.1 dynamic_slice.42
  51.3 0.3 fusion.40
  51.7 0.7 copy.26
  52.4 0.4 reshape.151
  52.8 0.1 convert_bitcast_fusion
  52.9 0.7 copy.28
  53.6 0.4 reshape.152
  54.0 11.3 %all-to-all-done.2 = bf16[1,128,4,512]{3,1,0,2:T(8,128)(2,1)} async-done(((bf16[1,128,4,512]{3,1,0,2:T(8,128)(2,1)}), bf16[1,128,4,512]{3,1,0,2:T(8,128)(2,1)}, u32[]{:S(2)}, u32[]{:S(2)}) %all-to-all-start.2) | async-done | bytes 524320 | tf_op jit(solution)/shard_map/all_to_all | solution.py:103
  65.3 1.2 reshape.147
  66.6 0.1 multiply_reduce_fusion.2
  66.8 0.1 multiply_reduce_fusion.1
  67.0 0.3 multiply_multiply_fusion.1
  67.2 0.3 multiply_multiply_fusion
  67.5 0.3 subtract_convert_fusion
  67.9 1.1 pad_maximum_fusion
  69.0 26.1 %while.54 = (s32[]{:T(128)}, bf16[4,512,128]{1,2,0:T(8,128)(2,1)S(1)}, s32[4]{0:T(128)S(1)}, bf16[512,4,2,64]{0,3,2,1:T(8,128)(2,1)}, bf16[512,4,2,64]{0,3,2,1:T...) while((s32[]{:T(128)}, ...), condition=%wide.region_8.9_spmd, body=%wide.region_2.8_spmd.sunk | while | flops 138281984 | bytes 9979571 | solution.py:125
  69.0 0.6 dynamic_slice.79
  71.5 0.1 iota_compare_fusion.2
  71.6 2.0 %fusion.54 = (f32[2,512]{1,0:T(2,128)S(1)}, f32[2,512,512]{1,2,0:T(8,128)S(1)}) fusion(pred[512,512]{0,1:T(8,128)(4,1)S(1)} %iota_compare_fusion.2, bf16[512,4,2,64]{0,3,2,1:T(8,128)(2,1)} %get-tuple-element.419, s32[]{:T(128)S(6)} %select_n.36, bf16[512,4,2,64]{0,3,2,1:T(8,128)(2,1)} %get-tuple-element.420), kind=kOutput, calls=%fused_computation.57.clone.1 | convolution fusion | flops 69206528 | bytes 2626560 | tf_op jit(solution)/shard_map/while/body/eval_jaxpr/while/body/eval_jaxpr/sub | solution.py:72
  73.6 0.3 broadcast_divide_fusion.2
  73.9 0.6 dynamic_slice.80
  74.4 0.9 multiply_reduce_fusion.4
  75.4 0.1 fusion.55
  75.5 0.6 dynamic_slice.79
  78.0 0.1 iota_compare_fusion.2
  78.1 2.0 %fusion.54 = (f32[2,512]{1,0:T(2,128)S(1)}, f32[2,512,512]{1,2,0:T(8,128)S(1)}) fusion(pred[512,512]{0,1:T(8,128)(4,1)S(1)} %iota_compare_fusion.2, bf16[512,4,2,64]{0,3,2,1:T(8,128)(2,1)} %get-tuple-element.419, s32[]{:T(128)S(6)} %select_n.36, bf16[512,4,2,64]{0,3,2,1:T(8,128)(2,1)} %get-tuple-element.420), kind=kOutput, calls=%fused_computation.57.clone.1 | convolution fusion | flops 69206528 | bytes 2626560 | tf_op jit(solution)/shard_map/while/body/eval_jaxpr/while/body/eval_jaxpr/sub | solution.py:72
  80.1 0.3 broadcast_divide_fusion.2
  80.4 0.6 dynamic_slice.80
  81.0 0.9 multiply_reduce_fusion.4
  81.9 0.1 fusion.55
  82.0 0.6 dynamic_slice.79
  84.6 0.1 iota_compare_fusion.2
  84.7 2.0 %fusion.54 = (f32[2,512]{1,0:T(2,128)S(1)}, f32[2,512,512]{1,2,0:T(8,128)S(1)}) fusion(pred[512,512]{0,1:T(8,128)(4,1)S(1)} %iota_compare_fusion.2, bf16[512,4,2,64]{0,3,2,1:T(8,128)(2,1)} %get-tuple-element.419, s32[]{:T(128)S(6)} %select_n.36, bf16[512,4,2,64]{0,3,2,1:T(8,128)(2,1)} %get-tuple-element.420), kind=kOutput, calls=%fused_computation.57.clone.1 | convolution fusion | flops 69206528 | bytes 2626560 | tf_op jit(solution)/shard_map/while/body/eval_jaxpr/while/body/eval_jaxpr/sub | solution.py:72
  86.6 0.3 broadcast_divide_fusion.2
  86.9 0.6 dynamic_slice.80
  87.5 0.9 multiply_reduce_fusion.4
  88.4 0.1 fusion.55
  88.6 0.6 dynamic_slice.79
  91.1 0.1 iota_compare_fusion.2
  91.2 2.0 %fusion.54 = (f32[2,512]{1,0:T(2,128)S(1)}, f32[2,512,512]{1,2,0:T(8,128)S(1)}) fusion(pred[512,512]{0,1:T(8,128)(4,1)S(1)} %iota_compare_fusion.2, bf16[512,4,2,64]{0,3,2,1:T(8,128)(2,1)} %get-tuple-element.419, s32[]{:T(128)S(6)} %select_n.36, bf16[512,4,2,64]{0,3,2,1:T(8,128)(2,1)} %get-tuple-element.420), kind=kOutput, calls=%fused_computation.57.clone.1 | convolution fusion | flops 69206528 | bytes 2626560 | tf_op jit(solution)/shard_map/while/body/eval_jaxpr/while/body/eval_jaxpr/sub | solution.py:72
  93.1 0.3 broadcast_divide_fusion.2
  93.4 0.6 dynamic_slice.80
  94.0 0.9 multiply_reduce_fusion.4
  95.0 0.1 fusion.55
  95.1 0.9 copy.32
  96.0 0.5 broadcast.175
  96.5 3.8 %reduce = bf16[512,512]{1,0:T(8,128)(2,1)S(1)} reduce(bf16[512,1,1,512]{3,2,1,0:T(2,128)(2,1)S(1)} %bitcast.87, bf16[]{:T(256)} %broadcast.175), dimensions={1,2}, to_apply=%bitcast.59.reduce_sub_computation | reduce | bytes 1048578
  100.3 0.4 reshape.155
  100.7 16.4 %all_to_all.48 = bf16[4,2,32768]{2,1,0:T(2,128)(2,1)S(1)} all-to-all(bf16[4,2,32768]{2,1,0:T(2,128)(2,1)S(1)} %reshape.155), channel_id=1, replica_groups=mesh['grp'=2,'sp'=4,'dp'=4] {'sp'}, dimensions={0} | all-to-all | bytes 1048576 | tf_op jit(solution)/shard_map/all_to_all | solution.py:127
  117.1 0.5 reshape.156
  117.7 0.1 copy.34
  117.8 0.3 copy.33
  118.1 5.5 %fusion.38 = bf16[1,128,2048]{2,1,0:T(8,128)(2,1)} fusion(bf16[128,2048]{0,1:T(8,128)(2,1)S(1)} %bitcast.85, bf16[2048,2048]{1,0:T(8,128)(2,1)} %all-gather.2.cloned.1.call-done), kind=kOutput, calls=%fused_computation.38 | convolution fusion | flops 1074003968 | bytes 9437184 | tf_op jit(solution)/shard_map/dot_general | solution.py:129
  (28 shorter events, 0.3 us)
Async XLA Ops:
  6.5 1.0 copy-start.1
  6.5 8.4 %copy-start.2 = (bf16[1,128,2048]{2,1,0:T(8,128)(2,1)S(1)}, bf16[1,128,2048]{2,1,0:T(8,128)(2,1)}, u32[]{:S(2)}) copy-start(bf16[1,128,2048]{2,1,0:T(8,128)(2,1)} %param.12) | copy-start | bytes 1572868
  6.5 111.5 %all-gather.2.cloned.1.call-start = ((), (), s32[]{:S(2)}) async-start(), calls=%async_computation.4 | async-start | bytes 10485760 | tf_op jit(solution)/shard_map/all_gather | solution.py:131
  7.6 25.5 %copy-start.3 = (bf16[1,128,2048]{2,1,0:T(8,128)(2,1)S(1)}, bf16[1,128,2048]{2,1,0:T(8,128)(2,1)}, u32[]{:S(2)}) copy-start(bf16[1,128,2048]{2,1,0:T(8,128)(2,1)} %param.14) | copy-start | bytes 1572868
  8.6 20.8 %all-to-all-start = ((bf16[1,128,4,512]{1,3,0,2:T(8,128)(2,1)}), bf16[1,128,4,512]{1,3,0,2:T(8,128)(2,1)S(1)}, u32[]{:S(2)}, u32[]{:S(2)}) async-start(bf16[1,128,4,512]{1,3,0,2:T(8,128)(2,1)} %bitcast.7), calls=%async_computation | async-start | bytes 1048576 | tf_op jit(solution)/shard_map/all_to_all | solution.py:102
  29.5 21.8 %copy-start.7 = (f32[16]{0:T(128)S(1)}, f32[16]{0:T(128)}, u32[]{:S(2)}) copy-start(f32[16]{0:T(128)} %param.17) | copy-start | bytes 196
  29.5 17.6 %all-to-all-start.1 = ((bf16[1,128,4,512]{1,3,0,2:T(8,128)(2,1)}), bf16[1,128,4,512]{1,3,0,2:T(8,128)(2,1)S(1)}, u32[]{:S(2)}, u32[]{:S(2)}) async-start(bf16[1,128,4,512]{1,3,0,2:T(8,128)(2,1)} %bitcast.10), calls=%async_computation.1 | async-start | bytes 1048576 | tf_op jit(solution)/shard_map/all_to_all | solution.py:101
  47.1 18.2 %all-to-all-start.2 = ((bf16[1,128,4,512]{3,1,0,2:T(8,128)(2,1)}), bf16[1,128,4,512]{3,1,0,2:T(8,128)(2,1)}, u32[]{:S(2)}, u32[]{:S(2)}) async-start(bf16[1,128,4,512]{3,1,0,2:T(8,128)(2,1)} %copy.30), calls=%async_computation.2 | async-start | bytes 1048576 | tf_op jit(solution)/shard_map/all_to_all | solution.py:103
  65.3 1.6 %copy-start.5 = (f32[64]{0:T(128)S(1)}, f32[64]{0:T(128)}, u32[]{:S(2)}) copy-start(f32[64]{0:T(128)} %param.16) | copy-start | bytes 772
  66.6 0.7 copy-start.6
  67.5 1.5 %copy-start = (bf16[4,512,128]{1,2,0:T(8,128)(2,1)S(1)}, bf16[4,512,128]{1,2,0:T(8,128)(2,1)}, u32[]{:S(2)}) copy-start(bf16[4,512,128]{1,2,0:T(8,128)(2,1)} %custom-call) | copy-start | bytes 1572868
  67.5 1.5 %copy-start.4 = (f32[128]{0:T(128)S(1)}, f32[128]{0:T(128)}, u32[]{:S(2)}) copy-start(f32[128]{0:T(128)} %param.18) | copy-start | bytes 1540
Sparse Core Ops, SparseCore 0:
  8.9 60.9 all-gather.1
where the time goes:
time: 131 us; the launch traced here: 130 us
  waiting for transfers between devices  38.2 us (29%)
  matrix products  17.1 us (13%)
  blocking collectives  16.4 us (13%)
  local copies, waits for them, and re-layouts  14.6 us (11%)
  starting transfers between devices  14.1 us (11%)
  between operations  13.6 us (10%)
  other arithmetic  8.36 us (6%)
  loops' own time  7.96 us (6%)
    all_to_all x1, blocking collectives, local(): lax.all_to_all(outputs, 'sp', split_axis=1, concat_axis=2, tiled=True)  16.4 us
    all_to_all x1, waiting for transfers between devices, local(): lax.all_to_all(by_peer(key_rows), 'sp', split_axis=2, concat_axis=1, tile...  13.5 us
    all_to_all x1, waiting for transfers between devices, local(): lax.all_to_all(by_peer(query_rows), 'sp', split_axis=2, concat_axis=1, ti...  12.7 us
    all_to_all x1, waiting for transfers between devices, local(): lax.all_to_all(by_peer(value_rows), 'sp', split_axis=2, concat_axis=1, ti...  11.3 us
    another operation x1, loops' own time, local(): outputs = lax.map(per_head, jnp.arange(local_heads, dtype=jnp.int32))  7.96 us
    sub x4, matrix products, one_block(): totals = jnp.sum(jnp.exp(stored - highest[..., None]), axis=-1)  7.85 us
    all_to_all x1, starting transfers between devices, local(): lax.all_to_all(by_peer(key_rows), 'sp', split_axis=2, concat_axis=1, tile...  6.35 us
    dot_general x1, matrix products, local(): jnp.dot(heads_rows, lax.all_gather(out_weight, 'dp', axis=1, tiled=True),...  5.46 us
  transfers between devices with their start and end apart: 4, of which 3 were waited for; matrix products, arithmetic and copies ran while one was open for 26% of the time, Pallas kernels for 0%

commit v1 on v0

v1 whole, which is shorter than its diff:
```python
import functools
import math

import jax
import jax.numpy as jnp
import numpy as np
from jax import lax
from jax.experimental import pallas as pl
from jax.experimental.pallas import tpu as pltpu
from jax.sharding import PartitionSpec as P

EPSILON = 1e-06
OUT_SCALE = 0.8
CHUNK_PARTS = (1, 1)
FIRST_GROUP = 3 / 8
MIB = 1024 * 1024


VMEM_SPEC = pl.BlockSpec(memory_space=pltpu.VMEM)
HBM_SPEC = pl.BlockSpec(memory_space=pltpu.HBM)
SMEM_SPEC = pl.BlockSpec(memory_space=pltpu.SMEM)
QUERY, KEY, VALUE = range(3)


class Plan:
    def __init__(self, n, owners, heads):
        self.n, self.owners, self.heads = n, owners, heads
        inward, back = {}, {}
        self.jobs = {device: [] for device in range(n)}
        for group, owner in enumerate(owners):
            for block in range(n):
                self.jobs[min(block, owner)].append((group, block))
                if block > owner:
                    inward.setdefault((block, owner), []).append((group, QUERY))
                    back.setdefault((owner, block), []).append(group)
                for target in range(block + 1, owner + 1):
                    inward.setdefault((block, target), []).append((group, KEY))
        self.ins = self.rounds(inward, lambda part: (3 - part[1]) * heads[part[0]])
        self.outs = self.rounds(back, lambda group: heads[group])

    def rounds(self, flows, slabs):
        sized = sorted(flows.items(), key=lambda flow: -sum(map(slabs, flow[1])))
        rounds = []
        for (source, target), parts in sized:
            places, count = [], 0
            for part in parts:
                places.append((part, count))
                count += slabs(part)
            for members in rounds:
                if all(source != other[0] and target != other[1] for other in members[1]):
                    members[1].append((source, target, places))
                    break
            else:
                rounds.append((count, [(source, target, places)]))
        return rounds

    def source_of(self, rounds, source, target, wanted):
        for number, (_, members) in enumerate(rounds):
            for member_source, member_target, places in members:
                if (member_source, member_target) == (source, target):
                    for part, first in places:
                        if part == wanted:
                            return number, first
        raise KeyError(wanted)


def pairs_of(members):
    return [(source, target) for source, target, _ in members]


def send_buffers(plan, rows, tables, gains, first_heads, width):
    groups = len(plan.owners)
    tokens = rows[0].shape[0]
    half = width // 2

    def body(*refs):
        row_refs, refs = refs[:3], refs[3:]
        cos_table, sin_table, query_gain_ref, key_gain_ref, *refs = refs
        own, refs = refs[:groups], refs[groups:]
        buffers, refs = refs[: len(plan.ins)], refs[len(plan.ins) :]
        staged, (cos_here, sin_here, query_gain, key_gain, sems) = refs[:groups], refs[groups:]
        me = lax.axis_index("sp")
        here = pl.ds(pl.multiple_of(me * tokens, tokens), tokens)
        copies = [
            pltpu.make_async_copy(cos_table.at[here, :], cos_here, sems.at[0]),
            pltpu.make_async_copy(sin_table.at[here, :], sin_here, sems.at[1]),
            pltpu.make_async_copy(query_gain_ref, query_gain, sems.at[2]),
            pltpu.make_async_copy(key_gain_ref, key_gain, sems.at[3]),
        ]
        for group in range(groups):
            lanes = pl.ds(first_heads[group] * width, plan.heads[group] * width)
            for part in range(3):
                copies.append(
                    pltpu.make_async_copy(
                        row_refs[part].at[:, lanes], staged[group].at[part], sems.at[len(copies)]
                    )
                )
        for copy in copies:
            copy.start()

        row = lax.broadcasted_iota(jnp.int32, (width, width), 0)
        column = lax.broadcasted_iota(jnp.int32, (width, width), 1)
        same_map = row // half == column // half
        sum_matrix = same_map.astype(jnp.bfloat16)
        sum_twice = jnp.concatenate([sum_matrix, sum_matrix], axis=0)
        pair_matrix = (same_map & (jnp.abs(row - column) == half // 2)).astype(jnp.bfloat16)
        for copy in copies:
            copy.wait()
        both_gains = [
            jnp.concatenate([ref[...], ref[...]], axis=1) for ref in (query_gain, key_gain)
        ]

        for part, gain in enumerate(both_gains):
            straight = cos_here[...] * gain
            crossed = sin_here[...] * pltpu.roll(gain, half // 2, 1)
            for group in range(groups):
                for head in range(plan.heads[group]):
                    field = staged[group][part, :, head * width : (head + 1) * width]
                    wide = field.astype(jnp.float32)
                    square = wide * wide
                    high = square.astype(jnp.bfloat16)
                    low = (square - high.astype(jnp.float32)).astype(jnp.bfloat16)
                    total = jnp.dot(
                        jnp.concatenate([high, low], axis=1), sum_twice, preferred_element_type=jnp.float32
                    )
                    pair = jnp.dot(field, pair_matrix, preferred_element_type=jnp.float32)
                    turned = wide * straight + pair * crossed
                    turned *= lax.rsqrt(total * (1.0 / half) + EPSILON)
                    own[group][part * plan.heads[group] + head] = turned.astype(jnp.bfloat16)
        for group in range(groups):
            for head in range(plan.heads[group]):
                own[group][VALUE * plan.heads[group] + head] = staged[group][
                    VALUE, :, head * width : (head + 1) * width
                ]

        for number, (_, members) in enumerate(plan.ins):
            for source, _, places in members:

                @pl.when(me == source)
                def _(number=number, places=places):
                    for (group, part), first in places:
                        skip = part * plan.heads[group]
                        count = 3 * plan.heads[group] - skip

                        def move(slab, carry, group=group, skip=skip, first=first):
                            buffers[number][first + slab] = own[group][skip + slab]
                            return carry

                        lax.fori_loop(0, count, move, 0, unroll=True)

    slabs = [3 * heads for heads in plan.heads] + [count for count, _ in plan.ins]
    results = pl.pallas_call(
        body,
        out_shape=[jax.ShapeDtypeStruct((count, tokens, width), jnp.bfloat16) for count in slabs],
        in_specs=[HBM_SPEC] * 7,
        out_specs=[VMEM_SPEC] * len(slabs),
        scratch_shapes=[pltpu.VMEM((3, tokens, heads * width), jnp.bfloat16) for heads in plan.heads]
        + [pltpu.VMEM((tokens, width), jnp.float32)] * 2
        + [pltpu.VMEM(gains[0].shape, jnp.float32)] * 2
        + [pltpu.SemaphoreType.DMA((4 + 3 * groups,))],
        compiler_params=pltpu.CompilerParams(vmem_limit_bytes=16 * MIB),
        name="pack",
    )(*rows, *tables, *gains)
    return results[:groups], results[groups:]


def attention(plan, own, arrived, lambdas, head_gain, first_heads):
    groups = len(plan.owners)
    tokens = own[0].shape[1]
    width = head_gain.shape[-1]
    half = width // 2
    exponent_scale = half ** (-0.5) * math.log2(math.e)
    unrolled = plan.n <= 4

    def body(lambda_ref, head_gain_ref, *refs):
        own_refs, refs = refs[:groups], refs[groups:]
        in_refs, refs = refs[: len(plan.ins)], refs[len(plan.ins) :]
        own_out, outs = refs[:groups], refs[groups:]
        me = lax.axis_index("sp")

        def block_of(device, group, part, head, slot):
            if slot == device:
                return own_refs[group][part * plan.heads[group] + head]
            lowest = QUERY if slot > plan.owners[group] else KEY
            number, first = plan.source_of(plan.ins, slot, device, (group, lowest))
            return in_refs[number][first + (part - lowest) * plan.heads[group] + head]

        def job(device, group, block, heads, gain, weight_of, store):
            slots = range(block + 1)
            first_map = lax.broadcasted_iota(jnp.int32, (tokens, width), 1) < half
            key_at = lax.broadcasted_iota(jnp.int32, (tokens, 2 * tokens), 0)
            query_at = lax.broadcasted_iota(jnp.int32, (tokens, 2 * tokens), 1) % tokens
            visible = key_at <= query_at

            maps, scores, values = [], [], []
            for head in heads:
                query = block_of(device, group, QUERY, head, block)
                zero = jnp.zeros_like(query)
                maps.append(
                    jnp.concatenate(
                        [jnp.where(first_map, query, zero), jnp.where(first_map, zero, query)], axis=0
                    )
                )
                values.append(
                    jnp.concatenate([block_of(device, group, VALUE, head, slot) for slot in slots], axis=0)
                )
            for head, query in zip(heads, maps):
                keys = jnp.concatenate([block_of(device, group, KEY, head, slot) for slot in slots], axis=0)
                product = lax.dot_general(
                    keys, query, (((1,), (1,)), ((), ())), preferred_element_type=jnp.float32
                )
                last = jnp.where(visible, product[block * tokens :], -1e30)
                scores.append(
                    jnp.concatenate([product[: block * tokens], last], axis=0) if block else last
                )
            highest = [jnp.max(part, axis=0, keepdims=True) for part in scores]
            exponents = [
                jnp.exp2((part - top) * exponent_scale) for part, top in zip(scores, highest)
            ]
            inverses = [1.0 / jnp.sum(part, axis=0, keepdims=True) for part in exponents]
            raws = []
            for head, exponent, inverse, value in zip(heads, exponents, inverses, values):
                mixing = (
                    exponent[:, :tokens] * inverse[:, :tokens]
                    - exponent[:, tokens:] * (inverse[:, tokens:] * weight_of(head))
                ).astype(jnp.bfloat16)
                raws.append(
                    lax.dot_general(
                        value, mixing, (((0,), (0,)), ((), ())), preferred_element_type=jnp.float32
                    )
                )
            for head, raw in zip(heads, raws):
                scaled = raw * lax.rsqrt(jnp.mean(raw * raw, axis=0, keepdims=True) + EPSILON)
                store(head, (scaled * gain).astype(jnp.bfloat16))

        for device, jobs in plan.jobs.items():
            if not jobs:
                continue

            @pl.when(me == device)
            def _(device=device, jobs=jobs):
                gain = jnp.transpose(
                    jnp.broadcast_to(head_gain_ref[...] * OUT_SCALE, (tokens, width))
                )
                for group, block in jobs:
                    if block == device:
                        target, first = own_out[group], 0
                    else:
                        number, first = plan.source_of(plan.outs, device, block, group)
                        target = outs[number]

                    def store(head, value, target=target, first=first):
                        target[first + head] = value

                    def weight_of(head, group=group):
                        return lambda_ref[first_heads[group] + head]

                    heads = plan.heads[group]
                    if unrolled:
                        job(device, group, block, range(heads), gain, weight_of, store)
                    else:

                        def one(head, carry, group=group, block=block, store=store, weight_of=weight_of):
                            job(device, group, block, [head], gain, weight_of, store)
                            return carry

                        lax.fori_loop(0, heads, one, 0)

    slabs = list(plan.heads) + [count for count, _ in plan.outs]
    results = pl.pallas_call(
        body,
        out_shape=[jax.ShapeDtypeStruct((count, width, tokens), jnp.bfloat16) for count in slabs],
        in_specs=[SMEM_SPEC] + [VMEM_SPEC] * (1 + groups + len(plan.ins)),
        out_specs=[VMEM_SPEC] * len(slabs),
        compiler_params=pltpu.CompilerParams(vmem_limit_bytes=(24 if unrolled else 48) * MIB),
        name="attend",
    )(lambdas, head_gain, *own, *arrived)
    return results[:groups], results[groups:]


def project(plan, own_heads, back, shards, total, first_heads, last, dtype):
    groups = len(plan.owners)
    _, width, tokens = own_heads[0].shape
    shard_columns = shards[0].shape[1]
    count = len(shards)
    given = 0 if total is None else 1
    starts = [sum(plan.heads[:group]) for group in range(groups)]

    def body(*refs):
        own_refs, refs = refs[:groups], refs[groups:]
        back_refs, refs = refs[: len(plan.outs)], refs[len(plan.outs) :]
        total_refs, refs = refs[:given], refs[given:]
        shard_refs, refs = refs[:count], refs[count:]
        out_ref, heads = refs
        me, column_place = lax.axis_index("sp"), lax.axis_index("dp")

        def take(ref, first, group):
            for head in range(plan.heads[group]):
                lanes = slice((starts[group] + head) * width, (starts[group] + head + 1) * width)
                heads[:, lanes] = jnp.transpose(ref[first + head])

        for group, owner in enumerate(plan.owners):
            pl.when(me <= owner)(functools.partial(take, own_refs[group], 0, group))
        for number, (_, members) in enumerate(plan.outs):
            for _, target, places in members:
                for group, first in places:
                    pl.when(me == target)(functools.partial(take, back_refs[number], first, group))

        for number in range(count):
            part = total_refs[0][number] if given else 0.0
            for group in range(groups):
                lanes = slice(starts[group] * width, (starts[group] + plan.heads[group]) * width)
                row = first_heads[group] * width
                part += jnp.dot(
                    heads[:, lanes],
                    shard_refs[number][row : row + plan.heads[group] * width, :],
                    preferred_element_type=jnp.float32,
                )
            if last:
                column = pl.multiple_of(shard_place(column_place, number, count) * shard_columns, shard_columns)
                out_ref[:, pl.ds(column, shard_columns)] = part.astype(dtype)
            else:
                out_ref[number] = part

    if last:
        out_shape = jax.ShapeDtypeStruct((tokens, count * shard_columns), dtype)
    else:
        out_shape = jax.ShapeDtypeStruct((count, tokens, shard_columns), jnp.float32)
    return pl.pallas_call(
        body,
        out_shape=out_shape,
        in_specs=[VMEM_SPEC] * (groups + len(plan.outs) + given + count),
        out_specs=VMEM_SPEC,
        scratch_shapes=[pltpu.VMEM((tokens, sum(plan.heads) * width), jnp.bfloat16)],
        compiler_params=pltpu.CompilerParams(vmem_limit_bytes=24 * MIB),
        name="project",
    )(*own_heads, *back, *([] if total is None else [total]), *shards)


def shard_place(place, number, count):
    if count & (count - 1) == 0:
        return jnp.bitwise_xor(place, number)
    return lax.rem(place + number, count)


def gather_shards(weight, hold):
    count = lax.axis_size("dp")
    if count & (count - 1):
        return [weight] + [
            lax.ppermute(weight, "dp", [(j, (j - k) % count) for j in range(count)])
            for k in range(1, count)
        ]
    shards, mask = {0: weight}, count // 2
    while mask:
        pairs = [(j, j ^ mask) for j in range(count)]
        sent = {}
        for k, shard in shards.items():
            sent[k ^ mask] = lax.ppermute(hold(shard) if k else shard, "dp", pairs)
        shards.update(sent)
        mask //= 2
    return [shards[k] for k in range(count)]


def rotation_tables(length, head_size):
    half_size = head_size // 2
    positions = np.arange(length, dtype=np.float32)
    inverse = np.float32(10000.0) ** (-np.arange(half_size, dtype=np.float32) / np.float32(half_size))
    angles = (positions[:, None] * inverse[None, :]).astype(np.float64)
    cosine_part, sine_part = np.cos(angles), np.sin(angles)
    return [
        in_hbm(jnp.asarray(np.concatenate(parts, axis=1).astype(np.float32)))
        for parts in ([cosine_part] * 4, [-sine_part, sine_part] * 2)
    ]


def bounds_of(heads):
    parts = len(CHUNK_PARTS)
    return [heads * sum(CHUNK_PARTS[:k]) // sum(CHUNK_PARTS) for k in range(parts + 1)]


def in_hbm(array):
    return pltpu.with_memory_space_constraint(array, pltpu.HBM)


def tie(array, other):
    return lax.optimization_barrier((array, other))[0]


def local(query_rows, key_rows, value_rows, query_gain, key_gain, lambdas, head_gain, out_weight):
    tokens = query_rows.shape[1]
    n = lax.axis_size("sp")
    owners = sorted({max(n // 2 - 1, 0), n // 2})
    heads_total = lambdas.shape[0]
    head_size, width = query_gain.shape[0], head_gain.shape[0]
    rows = [
        in_hbm(array.reshape(tokens, array.shape[2])) for array in (query_rows, key_rows, value_rows)
    ]
    first_count = max(1, int(heads_total * FIRST_GROUP)) if len(owners) > 1 else heads_total
    group_starts = [0, first_count][: len(owners)]
    group_bounds = [bounds_of(first_count), bounds_of(heads_total - first_count)][: len(owners)]
    chunks = []
    for k in range(len(CHUNK_PARTS)):
        heads = [bounds[k + 1] - bounds[k] for bounds in group_bounds]
        chunks.append(
            (Plan(n, owners, heads), [start + bounds[k] for start, bounds in zip(group_starts, group_bounds)])
        )

    tables = rotation_tables(tokens * n, head_size)
    gains = [in_hbm(gain.reshape(1, head_size)) for gain in (query_gain, key_gain)]
    head_gain = head_gain.reshape(1, width)
    own, arrived = [], []
    for plan, first_heads in chunks:
        if own:
            gains[0] = in_hbm(tie(gains[0], own[-1][0]))
        slabs, buffers = send_buffers(plan, rows, tables, gains, first_heads, width)
        own.append(slabs)
        arrived.append([lax.ppermute(buffer, "sp", pairs_of(flows)) for buffer, (_, flows) in zip(buffers, plan.ins)])
    attended = []
    for number, (plan, first_heads) in enumerate(chunks):
        head_gain = tie(head_gain, attended[-1][0][0] if attended else own[-1][0])
        own_heads, outward = attention(
            plan, own[number], arrived[number], lambdas, head_gain, first_heads
        )
        back = [
            lax.ppermute(buffer, "sp", pairs_of(flows)) for buffer, (_, flows) in zip(outward, plan.outs)
        ]
        attended.append((own_heads, back))
    shards = gather_shards(out_weight, lambda shard: tie(shard, attended[-1][0][0]))
    total = None
    for number, (plan, first_heads) in enumerate(chunks):
        total = project(
            plan, *attended[number], shards, total, first_heads, number == len(chunks) - 1, query_rows.dtype
        )
    return total.reshape(1, tokens, total.shape[1])


def solution(mesh):
    placed = (
        P(("grp", "dp"), "sp", None),
        P(("grp", "dp"), "sp", None),
        P(("grp", "dp"), "sp", None),
        P(),
        P(),
        P(),
        P(),
        P(None, "dp"),
    )

    return jax.shard_map(local, mesh=mesh, in_specs=placed, out_specs=P(("grp", "dp"), "sp", None), check_vma=False)
```

time: 131 us -> 66.9 us (0.51)
  the two profiles are of different devices: /device:TPU:0 before, /device:TPU:30 now
where the time goes in v1:
time: 66.9 us; the launch traced here: 66.6 us
  waiting for transfers between devices  34.1 us (51%)
  starting transfers between devices  23.7 us (35%)
  Pallas kernels  8.57 us (13%)
    ppermute x10, waiting for transfers between devices, local(): lax.ppermute(buffer, 'sp', pairs_of(flows))  29.8 us
    ppermute x10, starting transfers between devices, local(): lax.ppermute(buffer, 'sp', pairs_of(flows))  23.2 us
    pallas_call x2, Pallas kernels, send_buffers(): pl.pallas_call(body, out_shape=[jax.ShapeDtypeStruct((count, tokens, widt...  4.38 us
    ppermute x3, waiting for transfers between devices, gather_shards(): sent[k ^ mask] = lax.ppermute(hold(shard) if k else shard, 'dp', pairs)  4.3 us
    pallas_call x2, Pallas kernels, project(): pl.pallas_call(body, out_shape=out_shape, in_specs=[VMEM_SPEC] * (groups...  2.88 us
  transfers between devices with their start and end apart: 13, of which 7 were waited for; matrix products, arithmetic and copies ran while one was open for 0% of the time, Pallas kernels for 10%

profile of v1, /device:TPU:30, one launch (start us, length us, event | category | flops | bytes accessed | tf_op | source)
XLA Modules:
  0.0 66.6 jit_solution(280601877163165183)
XLA Ops:
  0.0 0.5 collective-permute-start.11
  0.5 0.0 copy-start
  0.5 0.0 copy-start.1
  0.5 0.0 copy-start.2
  0.5 2.3 %pack.2 = (bf16[9,128,128]{2,1,0:T(8,128)(2,1)S(1)}, bf16[15,128,128]{2,1,0:T(8,128)(2,1)S(1)}, bf16[16,128,128]{2,1,0:T(8,128)(2,1)S(1)}, bf16[10,128,128]{2,1,0:T(8,128)(2,1)S(1)}, bf16[10,128,128]{2,1,0:T(8,128)(2,1)S(1)}) custom-call(bf16[128,2048]{1,0:T(8,128)(2,1)} %bitcast.9, bf16[128,2048]{1,0:T(8,128)(2,1)} %bitcast.11, bf16[128,2048]{1,0:T(8,128)(2,1)} %bitcast.13, ...), custom_call_target="tpu_custom_call" | custom-call | tf_op jit(solution)/shard_map/pack/pallas_call | solution.py:152
  2.8 0.7 %collective-permute-start.1 = (bf16[10,128,128]{2,1,0:T(8,128)(2,1)S(1)}, bf16[10,128,128]{2,1,0:T(8,128)(2,1)S(1)}, u32[]{:S(2)}, u32[]{:S(2)}) collective-permute-start(bf16[10,128,128]{2,1,0:T(8,128)(2,1)S(1)} %get-tuple-element.33), channel_id=1, source_target_pairs={{0,8},{8,4},{1,9},{9,5},{2,10},{10,6},{3,11},{11,7},{16,24},{24,20... | collective-permute-start | bytes 983048 | tf_op jit(solution)/shard_map/ppermute | solution.py:417
  3.5 2.8 %collective-permute-start.2 = (bf16[10,128,128]{2,1,0:T(8,128)(2,1)S(1)}, bf16[10,128,128]{2,1,0:T(8,128)(2,1)S(1)}, u32[]{:S(2)}, u32[]{:S(2)}) collective-permute-start(bf16[10,128,128]{2,1,0:T(8,128)(2,1)S(1)} %get-tuple-element.34), channel_id=1, source_target_pairs={{4,8},{12,4},{5,9},{13,5},{6,10},{14,6},{7,11},{15,7},{20,24},{28,... | collective-permute-start | bytes 983048 | tf_op jit(solution)/shard_map/ppermute | solution.py:417
  6.3 2.5 %collective-permute-start = (bf16[16,128,128]{2,1,0:T(8,128)(2,1)S(1)}, bf16[16,128,128]{2,1,0:T(8,128)(2,1)S(1)}, u32[]{:S(2)}, u32[]{:S(2)}) collective-permute-start(bf16[16,128,128]{2,1,0:T(8,128)(2,1)S(1)} %get-tuple-element.32), channel_id=1, source_target_pairs={{0,4},{12,8},{1,5},{13,9},{2,6},{14,10},{3,7},{15,11},{16,20},{28,... | collective-permute-start | bytes 1572872 | tf_op jit(solution)/shard_map/ppermute | solution.py:417
  8.8 2.1 %pack.3 = (bf16[9,128,128]{2,1,0:T(8,128)(2,1)S(1)}, bf16[15,128,128]{2,1,0:T(8,128)(2,1)S(1)}, bf16[16,128,128]{2,1,0:T(8,128)(2,1)S(1)}, bf16[10,128,128]{2,1,0:T(8,128)(2,1)S(1)}, bf16[10,128,128]{2,1,0:T(8,128)(2,1)S(1)}) custom-call(bf16[128,2048]{1,0:T(8,128)(2,1)} %bitcast.10, bf16[128,2048]{1,0:T(8,128)(2,1)} %bitcast.12, ...), custom_call_target="tpu_custom_call" | custom-call | tf_op jit(solution)/shard_map/pack/pallas_call | solution.py:152
  11.0 1.3 %collective-permute-start.3 = (bf16[16,128,128]{2,1,0:T(8,128)(2,1)S(1)}, bf16[16,128,128]{2,1,0:T(8,128)(2,1)S(1)}, u32[]{:S(2)}, u32[]{:S(2)}) collective-permute-start(bf16[16,128,128]{2,1,0:T(8,128)(2,1)S(1)} %get-tuple-element.38), channel_id=1, source_target_pairs={{0,4},{12,8},{1,5},{13,9},{2,6},{14,10},{3,7},{15,11},{16,20},{28,... | collective-permute-start | bytes 1572872 | tf_op jit(solution)/shard_map/ppermute | solution.py:417
  12.3 0.0 collective-permute-done.1.refs_3_
  12.3 0.7 %collective-permute-start.4 = (bf16[10,128,128]{2,1,0:T(8,128)(2,1)S(1)}, bf16[10,128,128]{2,1,0:T(8,128)(2,1)S(1)}, u32[]{:S(2)}, u32[]{:S(2)}) collective-permute-start(bf16[10,128,128]{2,1,0:T(8,128)(2,1)S(1)} %get-tuple-element.39), channel_id=1, source_target_pairs={{0,8},{8,4},{1,9},{9,5},{2,10},{10,6},{3,11},{11,7},{16,24},{24,20... | collective-permute-start | bytes 983048 | tf_op jit(solution)/shard_map/ppermute | solution.py:417
  13.0 1.4 %collective-permute-done.2.refs_4_ = bf16[10,128,128]{2,1,0:T(8,128)(2,1)S(1)} collective-permute-done((bf16[10,128,128]{2,1,0:T(8,128)(2,1)S(1)}, bf16[10,128,128]{2,1,0:T(8,128)(2,1)S(1)}, u32[]{:S(2)}, u32[]{:S(2)}) %collective-permute-start.2) | collective-permute-done | bytes 327712 | tf_op jit(solution)/shard_map/ppermute | solution.py:417
  14.4 10.0 %collective-permute-start.5 = (bf16[10,128,128]{2,1,0:T(8,128)(2,1)S(1)}, bf16[10,128,128]{2,1,0:T(8,128)(2,1)S(1)}, u32[]{:S(2)}, u32[]{:S(2)}) collective-permute-start(bf16[10,128,128]{2,1,0:T(8,128)(2,1)S(1)} %get-tuple-element.40), channel_id=1, source_target_pairs={{4,8},{12,4},{5,9},{13,5},{6,10},{14,6},{7,11},{15,7},{20,24},{28,... | collective-permute-start | bytes 983048 | tf_op jit(solution)/shard_map/ppermute | solution.py:417
  24.4 1.2 %collective-permute-done.refs_2_ = bf16[16,128,128]{2,1,0:T(8,128)(2,1)S(1)} collective-permute-done((bf16[16,128,128]{2,1,0:T(8,128)(2,1)S(1)}, bf16[16,128,128]{2,1,0:T(8,128)(2,1)S(1)}, u32[]{:S(2)}, u32[]{:S(2)}) %collective-permute-start) | collective-permute-done | bytes 524320 | tf_op jit(solution)/shard_map/ppermute | solution.py:417
  25.6 0.0 copy-done
  25.6 0.0 collective-permute-start.10
  25.6 0.0 copy-done.1
  25.7 0.0 copy-done.2
  25.7 0.6 attend.2
  26.2 0.0 collective-permute-done.4.refs_3_
  26.2 16.3 %collective-permute-done.5.refs_4_ = bf16[10,128,128]{2,1,0:T(8,128)(2,1)S(1)} collective-permute-done((bf16[10,128,128]{2,1,0:T(8,128)(2,1)S(1)}, bf16[10,128,128]{2,1,0:T(8,128)(2,1)S(1)}, u32[]{:S(2)}, u32[]{:S(2)}) %collective-permute-start.5) | collective-permute-done | bytes 327712 | tf_op jit(solution)/shard_map/ppermute | solution.py:417
  42.5 0.0 collective-permute-done.3.refs_2_
  42.5 0.7 %attend.3 = (bf16[3,128,128]{2,1,0:T(8,128)(2,1)S(1)}, bf16[5,128,128]{2,1,0:T(8,128)(2,1)S(1)}, bf16[5,128,128]{2,1,0:T(8,128)(2,1)S(1)}, bf16[3,128,128]{2,1,0:T(8,128)(2,1)S(1)}) custom-call(f32[16]{0:T(128)S(1)} %copy-done.1, f32[1,128]{1,0:T(1,128)S(1)} %bitcast.8, bf16[9,128,128]{2,1,0:T(8,128)(2,1)S(1)} %get-tuple-element.29.refs_0_, ...), custom_call_target="tpu_custom_call" | custom-call | tf_op jit(solution)/shard_map/attend/pallas_call | solution.py:270
  43.3 4.3 %collective-permute-done.11.refs_6_.refs_7_ = bf16[2048,512]{1,0:T(8,128)(2,1)S(1)} collective-permute-done((bf16[2048,512]{1,0:T(8,128)(2,1)}, bf16[2048,512]{1,0:T(8,128)(2,1)S(1)}, u32[]{:S(2)}, u32[]{:S(2)}) %collective-permute-start.11) | collective-permute-done | bytes 2097184 | tf_op jit(solution)/shard_map/ppermute | solution.py:358
  47.6 0.0 collective-permute-start.12
  47.6 1.3 %collective-permute-start.9 = (bf16[3,128,128]{2,1,0:T(8,128)(2,1)S(1)}, bf16[3,128,128]{2,1,0:T(8,128)(2,1)S(1)}, u32[]{:S(2)}, u32[]{:S(2)}) collective-permute-start(bf16[3,128,128]{2,1,0:T(8,128)(2,1)S(1)} %get-tuple-element.47), channel_id=1, source_target_pairs={{4,12},{5,13},{6,14},{7,15},{20,28},{21,29},{22,30},{23,31}} | collective-permute-start | bytes 294920 | tf_op jit(solution)/shard_map/ppermute | solution.py:425
  48.9 1.3 %collective-permute-start.8 = (bf16[5,128,128]{2,1,0:T(8,128)(2,1)S(1)}, bf16[5,128,128]{2,1,0:T(8,128)(2,1)S(1)}, u32[]{:S(2)}, u32[]{:S(2)}) collective-permute-start(bf16[5,128,128]{2,1,0:T(8,128)(2,1)S(1)} %get-tuple-element.46), channel_id=1, source_target_pairs={{8,12},{4,8},{9,13},{5,9},{10,14},{6,10},{11,15},{7,11},{24,28},{2... | collective-permute-start | bytes 491528 | tf_op jit(solution)/shard_map/ppermute | solution.py:425
  50.2 1.3 %collective-permute-start.6 = (bf16[5,128,128]{2,1,0:T(8,128)(2,1)S(1)}, bf16[5,128,128]{2,1,0:T(8,128)(2,1)S(1)}, u32[]{:S(2)}, u32[]{:S(2)}) collective-permute-start(bf16[5,128,128]{2,1,0:T(8,128)(2,1)S(1)} %get-tuple-element.43), channel_id=1, source_target_pairs={{8,12},{4,8},{9,13},{5,9},{10,14},{6,10},{11,15},{7,11},{24,28},{2... | collective-permute-start | bytes 491528 | tf_op jit(solution)/shard_map/ppermute | solution.py:425
  51.5 4.6 %collective-permute-done.9.refs_3_ = bf16[3,128,128]{2,1,0:T(8,128)(2,1)S(1)} collective-permute-done((bf16[3,128,128]{2,1,0:T(8,128)(2,1)S(1)}, bf16[3,128,128]{2,1,0:T(8,128)(2,1)S(1)}, u32[]{:S(2)}, u32[]{:S(2)}) %collective-permute-start.9) | collective-permute-done | bytes 98336 | tf_op jit(solution)/shard_map/ppermute | solution.py:425
  56.0 1.3 %collective-permute-start.7 = (bf16[3,128,128]{2,1,0:T(8,128)(2,1)S(1)}, bf16[3,128,128]{2,1,0:T(8,128)(2,1)S(1)}, u32[]{:S(2)}, u32[]{:S(2)}) collective-permute-start(bf16[3,128,128]{2,1,0:T(8,128)(2,1)S(1)} %get-tuple-element.44), channel_id=1, source_target_pairs={{4,12},{5,13},{6,14},{7,15},{20,28},{21,29},{22,30},{23,31}} | collective-permute-start | bytes 294920 | tf_op jit(solution)/shard_map/ppermute | solution.py:425
  57.3 1.8 %collective-permute-done.8.refs_2_ = bf16[5,128,128]{2,1,0:T(8,128)(2,1)S(1)} collective-permute-done((bf16[5,128,128]{2,1,0:T(8,128)(2,1)S(1)}, bf16[5,128,128]{2,1,0:T(8,128)(2,1)S(1)}, u32[]{:S(2)}, u32[]{:S(2)}) %collective-permute-start.8) | collective-permute-done | bytes 163872 | tf_op jit(solution)/shard_map/ppermute | solution.py:425
  59.1 0.0 collective-permute-done.10.refs_5_.refs_6_
  59.1 0.0 collective-permute-done.12.refs_7_.refs_8_
  59.1 1.0 %project.2.refs_4_ = f32[4,128,512]{2,1,0:T(8,128)S(1)} custom-call(bf16[3,128,128]{2,1,0:T(8,128)(2,1)S(1)} %get-tuple-element.35.refs_0_, bf16[5,128,128]{2,1,0:T(8,128)(2,1)S(1)} %get-tuple-element.45.refs_1_, bf16[5,128,128]{2,1,0:T(8,128)(2,1)S(1)} %collective-permute-done.8.refs_2_, bf16[3,128,128]{2,1,0:T(8,128)(2,1)S(1)} %collective-permute-done.9.refs_3_, ...), custom_call_target="tpu_custom_call" | custom-call | tf_op jit(solution)/shard_map/project/pallas_call | solution.py:329
  60.2 4.5 %collective-permute-done.7.refs_3_ = bf16[3,128,128]{2,1,0:T(8,128)(2,1)S(1)} collective-permute-done((bf16[3,128,128]{2,1,0:T(8,128)(2,1)S(1)}, bf16[3,128,128]{2,1,0:T(8,128)(2,1)S(1)}, u32[]{:S(2)}, u32[]{:S(2)}) %collective-permute-start.7) | collective-permute-done | bytes 98336 | tf_op jit(solution)/shard_map/ppermute | solution.py:425
  64.7 0.0 collective-permute-done.6.refs_2_
  64.7 1.8 %project.3 = bf16[128,2048]{1,0:T(8,128)(2,1)} custom-call(bf16[3,128,128]{2,1,0:T(8,128)(2,1)S(1)} %get-tuple-element.41.refs_0_, bf16[5,128,128]{2,1,0:T(8,128)(2,1)S(1)} %get-tuple-element.42.refs_1_, bf16[5,128,128]{2,1,0:T(8,128)(2,1)S(1)} %collective-permute-done.6.refs_2_, bf16[3,128,128]{2,1,0:T(8,128)(2,1)S(1)} %collective-permute-done.7.refs_3_, ...), custom_call_target="tpu_custom_call" | custom-call | tf_op jit(solution)/shard_map/project/pallas_call | solution.py:329
Async XLA Ops:
  0.0 47.6 %collective-permute-start.11 = (bf16[2048,512]{1,0:T(8,128)(2,1)}, bf16[2048,512]{1,0:T(8,128)(2,1)S(1)}, u32[]{:S(2)}, u32[]{:S(2)}) collective-permute-start(bf16[2048,512]{1,0:T(8,128)(2,1)} %refs_5_.1), channel_id=1, source_target_pairs={{0,2},{1,3},{2,0},{3,1},{4,6},{5,7},{6,4},{7,5},{8,10},{9,11},{10,... | collective-permute-start | bytes 6291464 | tf_op jit(solution)/shard_map/ppermute | solution.py:358
  0.5 25.1 %copy-start = (bf16[2048,512]{1,0:T(8,128)(2,1)S(1)}, bf16[2048,512]{1,0:T(8,128)(2,1)}, u32[]{:S(2)}) copy-start(bf16[2048,512]{1,0:T(8,128)(2,1)} %refs_5_.1) | copy-start | bytes 6291460
  0.5 25.1 %copy-start.1 = (f32[16]{0:T(128)S(1)}, f32[16]{0:T(128)}, u32[]{:S(2)}) copy-start(f32[16]{0:T(128)} %lambda_ref.3) | copy-start | bytes 196
  0.5 25.1 %copy-start.2 = (f32[128]{0:T(128)S(1)}, f32[128]{0:T(128)}, u32[]{:S(2)}) copy-start(f32[128]{0:T(128)} %param.16) | copy-start | bytes 1540
  2.8 9.5 %collective-permute-start.1 = (bf16[10,128,128]{2,1,0:T(8,128)(2,1)S(1)}, bf16[10,128,128]{2,1,0:T(8,128)(2,1)S(1)}, u32[]{:S(2)}, u32[]{:S(2)}) collective-permute-start(bf16[10,128,128]{2,1,0:T(8,128)(2,1)S(1)} %get-tuple-element.33), channel_id=1, source_target_pairs={{0,8},{8,4},{1,9},{9,5},{2,10},{10,6},{3,11},{11,7},{16,24},{24,20... | collective-permute-start | bytes 983048 | tf_op jit(solution)/shard_map/ppermute | solution.py:417
  3.5 10.9 %collective-permute-start.2 = (bf16[10,128,128]{2,1,0:T(8,128)(2,1)S(1)}, bf16[10,128,128]{2,1,0:T(8,128)(2,1)S(1)}, u32[]{:S(2)}, u32[]{:S(2)}) collective-permute-start(bf16[10,128,128]{2,1,0:T(8,128)(2,1)S(1)} %get-tuple-element.34), channel_id=1, source_target_pairs={{4,8},{12,4},{5,9},{13,5},{6,10},{14,6},{7,11},{15,7},{20,24},{28,... | collective-permute-start | bytes 983048 | tf_op jit(solution)/shard_map/ppermute | solution.py:417
  6.3 19.3 %collective-permute-start = (bf16[16,128,128]{2,1,0:T(8,128)(2,1)S(1)}, bf16[16,128,128]{2,1,0:T(8,128)(2,1)S(1)}, u32[]{:S(2)}, u32[]{:S(2)}) collective-permute-start(bf16[16,128,128]{2,1,0:T(8,128)(2,1)S(1)} %get-tuple-element.32), channel_id=1, source_target_pairs={{0,4},{12,8},{1,5},{13,9},{2,6},{14,10},{3,7},{15,11},{16,20},{28,... | collective-permute-start | bytes 1572872 | tf_op jit(solution)/shard_map/ppermute | solution.py:417
  11.0 31.6 %collective-permute-start.3 = (bf16[16,128,128]{2,1,0:T(8,128)(2,1)S(1)}, bf16[16,128,128]{2,1,0:T(8,128)(2,1)S(1)}, u32[]{:S(2)}, u32[]{:S(2)}) collective-permute-start(bf16[16,128,128]{2,1,0:T(8,128)(2,1)S(1)} %get-tuple-element.38), channel_id=1, source_target_pairs={{0,4},{12,8},{1,5},{13,9},{2,6},{14,10},{3,7},{15,11},{16,20},{28,... | collective-permute-start | bytes 1572872 | tf_op jit(solution)/shard_map/ppermute | solution.py:417
  12.3 13.9 %collective-permute-start.4 = (bf16[10,128,128]{2,1,0:T(8,128)(2,1)S(1)}, bf16[10,128,128]{2,1,0:T(8,128)(2,1)S(1)}, u32[]{:S(2)}, u32[]{:S(2)}) collective-permute-start(bf16[10,128,128]{2,1,0:T(8,128)(2,1)S(1)} %get-tuple-element.39), channel_id=1, source_target_pairs={{0,8},{8,4},{1,9},{9,5},{2,10},{10,6},{3,11},{11,7},{16,24},{24,20... | collective-permute-start | bytes 983048 | tf_op jit(solution)/shard_map/ppermute | solution.py:417
  14.4 28.1 %collective-permute-start.5 = (bf16[10,128,128]{2,1,0:T(8,128)(2,1)S(1)}, bf16[10,128,128]{2,1,0:T(8,128)(2,1)S(1)}, u32[]{:S(2)}, u32[]{:S(2)}) collective-permute-start(bf16[10,128,128]{2,1,0:T(8,128)(2,1)S(1)} %get-tuple-element.40), channel_id=1, source_target_pairs={{4,8},{12,4},{5,9},{13,5},{6,10},{14,6},{7,11},{15,7},{20,24},{28,... | collective-permute-start | bytes 983048 | tf_op jit(solution)/shard_map/ppermute | solution.py:417
  25.6 33.5 %collective-permute-start.10 = (bf16[2048,512]{1,0:T(8,128)(2,1)S(1)}, bf16[2048,512]{1,0:T(8,128)(2,1)S(1)}, u32[]{:S(2)}, u32[]{:S(2)}) collective-permute-start(bf16[2048,512]{1,0:T(8,128)(2,1)S(1)} %copy-done), channel_id=1, source_target_pairs={{0,1},{1,0},{2,3},{3,2},{4,5},{5,4},{6,7},{7,6},{8,9},{9,8},{10,11... | collective-permute-start | bytes 6291464 | tf_op jit(solution)/shard_map/ppermute | solution.py:358
  47.6 11.5 %collective-permute-start.12 = (bf16[2048,512]{1,0:T(8,128)(2,1)S(1)}, bf16[2048,512]{1,0:T(8,128)(2,1)S(1)}, u32[]{:S(2)}, u32[]{:S(2)}) collective-permute-start(bf16[2048,512]{1,0:T(8,128)(2,1)S(1)} %collective-permute-done.11.refs_6_.refs_7_), channel_id=1, source_target_pairs={{0,1},{1,0},{2,3},{3,2},{4,5},{5,4},{6,7},{7,6},{8,9},{9,8},{10,11... | collective-permute-start | bytes 6291464 | tf_op jit(solution)/shard_map/ppermute | solution.py:358
  47.6 8.4 %collective-permute-start.9 = (bf16[3,128,128]{2,1,0:T(8,128)(2,1)S(1)}, bf16[3,128,128]{2,1,0:T(8,128)(2,1)S(1)}, u32[]{:S(2)}, u32[]{:S(2)}) collective-permute-start(bf16[3,128,128]{2,1,0:T(8,128)(2,1)S(1)} %get-tuple-element.47), channel_id=1, source_target_pairs={{4,12},{5,13},{6,14},{7,15},{20,28},{21,29},{22,30},{23,31}} | collective-permute-start | bytes 294920 | tf_op jit(solution)/shard_map/ppermute | solution.py:425
  48.9 10.2 %collective-permute-start.8 = (bf16[5,128,128]{2,1,0:T(8,128)(2,1)S(1)}, bf16[5,128,128]{2,1,0:T(8,128)(2,1)S(1)}, u32[]{:S(2)}, u32[]{:S(2)}) collective-permute-start(bf16[5,128,128]{2,1,0:T(8,128)(2,1)S(1)} %get-tuple-element.46), channel_id=1, source_target_pairs={{8,12},{4,8},{9,13},{5,9},{10,14},{6,10},{11,15},{7,11},{24,28},{2... | collective-permute-start | bytes 491528 | tf_op jit(solution)/shard_map/ppermute | solution.py:425
  50.2 14.5 %collective-permute-start.6 = (bf16[5,128,128]{2,1,0:T(8,128)(2,1)S(1)}, bf16[5,128,128]{2,1,0:T(8,128)(2,1)S(1)}, u32[]{:S(2)}, u32[]{:S(2)}) collective-permute-start(bf16[5,128,128]{2,1,0:T(8,128)(2,1)S(1)} %get-tuple-element.43), channel_id=1, source_target_pairs={{8,12},{4,8},{9,13},{5,9},{10,14},{6,10},{11,15},{7,11},{24,28},{2... | collective-permute-start | bytes 491528 | tf_op jit(solution)/shard_map/ppermute | solution.py:425
  56.0 8.7 %collective-permute-start.7 = (bf16[3,128,128]{2,1,0:T(8,128)(2,1)S(1)}, bf16[3,128,128]{2,1,0:T(8,128)(2,1)S(1)}, u32[]{:S(2)}, u32[]{:S(2)}) collective-permute-start(bf16[3,128,128]{2,1,0:T(8,128)(2,1)S(1)} %get-tuple-element.44), channel_id=1, source_target_pairs={{4,12},{5,13},{6,14},{7,15},{20,28},{21,29},{22,30},{23,31}} | collective-permute-start | bytes 294920 | tf_op jit(solution)/shard_map/ppermute | solution.py:425
